TPU v7x, 32 devices: a whole 2x2x4 slice. The times are simulated.
32 devices in a mesh: ep: 16 (over z, y, x), tp: 2 (over core).
Axes of the slice: x: 2, y: 2, z: 4, core: 2. Of those that a mesh axis runs over, the one named last changes fastest.
Arguments:
- residual: bfloat16 [256, 2048], P(('ep', 'tp')), may hold values from -6 to 6
- query_latent: bfloat16 [256, 8, 512], P(('ep', 'tp')), may hold values from -40 to 40
- query_rotary: bfloat16 [256, 8, 32], P(('ep', 'tp')), may hold values from -6 to 6
- latent_new: bfloat16 [256, 512], P(('ep', 'tp')), may hold values from -16 to 16
- rotary_new: bfloat16 [256, 32], P(('ep', 'tp')), may hold values from -6 to 6
- latent_cache: bfloat16 [256, 256, 512], P(('ep', 'tp')), may hold values from -16 to 16
- rotary_cache: bfloat16 [256, 256, 32], P(('ep', 'tp')), may hold values from -6 to 6
- lengths: int32 [256], P(('ep', 'tp')), may hold values from 32 to 256, as said below
- value_up: bfloat16 [512, 8, 64], replicated, may hold values from -1 to 1
- out_proj: bfloat16 [512, 2048], replicated, may hold values from -0.5 to 0.5
- attn_gain: bfloat16 [2048], replicated, may hold values from 0.099609375 to 1.8984375
- mix_gate: bfloat16 [2048], replicated, may hold values from -0.125 to 0.125
- dense_w_gate: bfloat16 [2048, 2048], P(None, 'ep'), may hold values from -0.125 to 0.125
- dense_w_up: bfloat16 [2048, 2048], P(None, 'ep'), may hold values from -0.125 to 0.125
- dense_w_down: bfloat16 [2048, 2048], P('ep'), may hold values from -0.5 to 0.5
- expert_ids: int32 [256, 6], P(('ep', 'tp')), may hold values from 0 to 15, all different within a row; in each aligned block of 16 rows (0 to 15, 16 to 31, ...) at most 12 rows name the same one
- expert_scores: float32 [256, 6], P(('ep', 'tp')), may hold values from 0.1 to 5
- expert_gate: bfloat16 [16, 2048, 512], P('ep', None, 'tp'), may hold values from -0.125 to 0.125
- expert_up: bfloat16 [16, 2048, 512], P('ep', None, 'tp'), may hold values from -0.125 to 0.125
- expert_down: bfloat16 [16, 512, 2048], P('ep', 'tp'), may hold values from -1 to 1
- out_gain: bfloat16 [2048], replicated, may hold values from 0.099609375 to 1.8984375
Outputs:
- layer_out: bfloat16 [256, 2048], P(('ep', 'tp'))
Inputs may be any that keep to these rules, and one draw needn't show every extreme that they name: `expert_ids`: within each aligned block of 16 rows (the sequences of one ep index) no expert is named by more than 12 rows, a bound that some block reaches; a row names 6 different experts. `lengths`: some sequence has exactly 256 cached positions.
All inputs are finite; a program needn't handle non-finite values.
Results may differ from a plain program's by a relative error of at most 0.018.
Values may be sent and summed in bfloat16 or wider, within the bound.
A program may use at most 128 MiB of HBM per device.

v0:
```python
import jax
import jax.numpy as jnp
from jax import lax
from jax.sharding import PartitionSpec as P

NOPE = 64


ALPHA = 8.0**0.25
EPS = 1e-06
ROPE_BASE = 10000.0


def rotate(vector, position):
    half_dim = vector.shape[-1] // 2
    inv_freq = ROPE_BASE ** (-jnp.arange(half_dim, dtype=jnp.float32) / half_dim)
    angles = position.astype(jnp.float32)[..., None] * inv_freq
    cosine = jnp.cos(angles)
    sine_part = jnp.sin(angles)
    lower_half = vector[..., :half_dim]
    upper_half = vector[..., half_dim:]
    return jnp.concatenate(
        [
            lower_half * cosine - upper_half * sine_part,
            upper_half * cosine + lower_half * sine_part,
        ],
        axis=-1,
    )


def normalize(values, gain):
    center = jnp.mean(values, -1, keepdims=True)
    spread = jnp.mean(jnp.square(values - center), -1, keepdims=True)
    return (values - center) * lax.rsqrt(spread + EPS) * gain.astype(jnp.float32)


def on_device(
    residual,
    query_latent,
    query_rotary,
    latent_new,
    rotary_new,
    latent_cache,
    rotary_cache,
    lengths,
    value_up,
    out_proj,
    attn_gain,
    mix_gate,
    dense_w_gate,
    dense_w_up,
    dense_w_down,
    expert_ids,
    expert_scores,
    expert_gate,
    expert_up,
    expert_down,
    out_gain,
):
    seq_count, model_width = residual.shape
    cache_len = latent_cache.shape[1]
    topk_count = expert_ids.shape[1]
    score_scale = (NOPE + query_rotary.shape[-1]) ** (-0.5)
    query_turned = rotate(query_rotary.astype(jnp.float32), lengths[:, None]).astype(jnp.bfloat16)
    key_turned = rotate(rotary_new.astype(jnp.float32), lengths).astype(jnp.bfloat16)
    scores = (
        jnp.einsum("bhr,btr->bht", query_latent, latent_cache, preferred_element_type=jnp.float32)
        + jnp.einsum("bhe,bte->bht", query_turned, rotary_cache, preferred_element_type=jnp.float32)
    ) * score_scale
    own_score = (
        jnp.einsum("bhr,br->bh", query_latent, latent_new, preferred_element_type=jnp.float32)
        + jnp.einsum("bhe,be->bh", query_turned, key_turned, preferred_element_type=jnp.float32)
    ) * score_scale
    live = jnp.arange(cache_len)[None, :] < lengths[:, None]
    scores = jnp.where(live[:, None, :], scores, -jnp.inf)
    top_score = jnp.maximum(jnp.max(scores, -1), own_score)
    cache_probs = jnp.exp(scores - top_score[..., None])
    own_prob = jnp.exp(own_score - top_score)
    prob_total = jnp.sum(cache_probs, -1) + own_prob
    cache_weights = (cache_probs / prob_total[..., None]).astype(jnp.bfloat16)
    own_weight = (own_prob / prob_total).astype(jnp.bfloat16)
    latent_out = (
        jnp.einsum("bht,btr->bhr", cache_weights, latent_cache, preferred_element_type=jnp.float32)
        + own_weight.astype(jnp.float32)[..., None] * latent_new.astype(jnp.float32)[:, None, :]
    ).astype(jnp.bfloat16)
    heads_out = jnp.einsum("bhr,rhv->bhv", latent_out, value_up, preferred_element_type=jnp.float32)
    heads_out = heads_out.astype(jnp.bfloat16).reshape(seq_count, -1)
    attn = jnp.dot(heads_out, out_proj, preferred_element_type=jnp.float32).astype(jnp.bfloat16)
    mixed = normalize(
        ALPHA * residual.astype(jnp.float32) + attn.astype(jnp.float32), attn_gain
    ).astype(jnp.bfloat16)
    mix = jax.nn.sigmoid(jnp.dot(mixed, mix_gate, preferred_element_type=jnp.float32))
    piece = lax.all_gather(mixed, "ep", axis=0, tiled=True)
    gate_pre = jnp.dot(piece, dense_w_gate, preferred_element_type=jnp.float32)
    up_pre = jnp.dot(piece, dense_w_up, preferred_element_type=jnp.float32)
    hidden_all = (jax.nn.silu(gate_pre) * up_pre).astype(jnp.bfloat16)
    dense_sum = lax.psum_scatter(
        jnp.dot(hidden_all, dense_w_down, preferred_element_type=jnp.float32),
        "ep",
        scatter_dimension=0,
        tiled=True,
    )
    dense_out = dense_sum.astype(jnp.bfloat16)
    group_rows, group_codes = (
        lax.all_gather(mixed, "tp", axis=0, tiled=True),
        lax.all_gather(expert_ids.astype(jnp.bfloat16), "tp", axis=0, tiled=True),
    )
    route_ids = group_codes.astype(jnp.int32).reshape(-1)
    group_tokens = group_rows.shape[0]
    expert_count = lax.axis_size("ep") * expert_gate.shape[0]
    slot_cap = max(2, 2 * group_tokens * topk_count // expert_count)
    onehot = (route_ids[:, None] == jnp.arange(expert_count, dtype=jnp.int32)[None, :]).astype(
        jnp.int32
    )
    slot_index = jnp.sum((jnp.cumsum(onehot, 0) - 1) * onehot, 1)
    outgoing = jnp.zeros((expert_count, slot_cap, model_width), jnp.bfloat16)
    outgoing = outgoing.at[route_ids, slot_index].set(jnp.repeat(group_rows, topk_count, axis=0))
    arrived = lax.all_to_all(outgoing, "ep", split_axis=0, concat_axis=0, tiled=True)
    sources, count, features = arrived.shape
    flat_rows = arrived.reshape(sources * count, features)
    gate_pre = jnp.dot(flat_rows, expert_gate[0], preferred_element_type=jnp.float32)
    up_pre = jnp.dot(flat_rows, expert_up[0], preferred_element_type=jnp.float32)
    hidden_part = (jax.nn.silu(gate_pre) * up_pre).astype(jnp.bfloat16)
    partial_value = jnp.dot(
        hidden_part, expert_down[0], preferred_element_type=jnp.float32
    ).reshape(sources, count, features)
    summed = lax.psum(partial_value.astype(jnp.bfloat16), "tp")
    returned = lax.all_to_all(summed, "ep", split_axis=0, concat_axis=0, tiled=True)
    own_slots = returned[route_ids, slot_index].reshape(group_tokens, topk_count, model_width)
    picked = lax.dynamic_slice_in_dim(own_slots, lax.axis_index("tp") * seq_count, seq_count, 0)
    route_share = expert_scores / jnp.sum(expert_scores, 1, keepdims=True)
    routed = jnp.sum(picked.astype(jnp.float32) * route_share[:, :, None], 1)
    summed_total = (
        ALPHA * mixed.astype(jnp.float32) + routed + mix[:, None] * dense_out.astype(jnp.float32)
    )
    return normalize(summed_total, out_gain).astype(jnp.bfloat16)


def solution(mesh):
    return jax.shard_map(
        on_device,
        mesh=mesh,
        in_specs=(
            P(("ep", "tp"), None),
            P(("ep", "tp"), None, None),
            P(("ep", "tp"), None, None),
            P(("ep", "tp"), None),
            P(("ep", "tp"), None),
            P(("ep", "tp"), None, None),
            P(("ep", "tp"), None, None),
            P(("ep", "tp")),
            P(),
            P(),
            P(),
            P(),
            P(None, "ep"),
            P(None, "ep"),
            P("ep", None),
            P(("ep", "tp"), None),
            P(("ep", "tp"), None),
            P("ep", None, "tp"),
            P("ep", None, "tp"),
            P("ep", "tp", None),
            P(),
        ),
        out_specs=P(("ep", "tp"), None),
        check_vma=False,
    )
```

profile of v0, /device:TPU:0, one launch (start us, length us, event | category | flops | bytes accessed | tf_op | source)
XLA Modules:
  0.0 203.4 jit_solution(17127304516886828509)
XLA Ops:
  7.4 0.9 iota_compare_fusion.1
  8.3 0.7 convert_element_type.101
  9.0 0.7 convert_element_type.87
  9.7 2.0 all_gather.9
  11.6 0.1 eq.15
  11.7 0.1 reshape.179
  11.8 0.7 convert_element_type.88
  12.5 0.7 convert_element_type.86
  13.2 0.7 convert_element_type.92
  13.9 1.5 fusion.45
  15.5 0.1 fusion.29
  15.6 0.1 subtract_convert_fusion.1
  15.9 0.2 fusion.31
  16.1 0.3 fusion.43
  16.4 0.2 fusion.24
  16.6 0.4 fusion.3
  17.0 0.2 fusion.8
  17.3 0.1 reshape.178
  17.4 2.1 %fusion.44 = (f32[8]{0:T(128)S(1)}, f32[8,2048]{1,0:T(8,128)S(1)}) fusion(bf16[8,512]{1,0:T(8,128)(2,1)S(1)} %reshape.178, bf16[512,2048]{1,0:T(8,128)(2,1)} %param.30, bf16[8,2048]{1,0:T(8,128)(2,1)S(1)} %copy-done.6), kind=kOutput, calls=%fused_computation.86 | convolution fusion | flops 16875512 | bytes 2203680 | tf_op jit(solution)/shard_map/dot_general | solution.py:88
  19.5 0.2 multiply_reduce_fusion.2
  19.7 0.1 multiply_convert_fusion.1
  19.8 1.9 all_gather.10
  21.7 0.1 reshape.191
  22.0 0.1 reduce_window_sum.11
  22.1 0.2 select_reduce_fusion
  22.4 9.0 %scatter_fusion = bf16[16,12,2048]{2,0,1:T(8,128)(2,1)S(1)} fusion(bf16[16,12,2048]{2,0,1:T(8,128)(2,1)S(1)} %broadcast_in_dim.18, s32[96]{0:T(128)S(1)} %get-tuple-element.7, bf16[96,2048]{1,0:T(8,128)(2,1)S(1)} %reshape.191), kind=kCustom, calls=%fused_computation.1 | custom fusion | bytes 1180416 | tf_op jit(solution)/shard_map/scatter | solution.py:117
  31.4 0.4 copy.30
  31.9 34.6 %all_to_all.10 = bf16[16,12,2048]{2,1,0:T(8,128)(2,1)S(1)} all-to-all(bf16[16,12,2048]{2,1,0:T(8,128)(2,1)S(1)} %copy.30), channel_id=1, replica_groups=mesh['ep'=16,'tp'=2] {'ep'}, dimensions={0} | all-to-all | bytes 1572864 | tf_op jit(solution)/shard_map/all_to_all | solution.py:118
  66.5 1.1 reshape.181
  67.6 1.9 fusion.15
  69.5 1.8 fusion.2
  71.4 1.3 convolution_convert_fusion
  72.8 41.5 %all_gather.11 = bf16[128,2048]{1,0:T(8,128)(2,1)S(1)} all-gather(bf16[8,2048]{1,0:T(8,128)(2,1)S(1)} %multiply_convert_fusion.1), channel_id=1, replica_groups=mesh['ep'=16,'tp'=2] {'ep'}, dimensions={0}, use_global_device_ids=true | all-gather | bytes 557056 | tf_op jit(solution)/shard_map/all_gather | solution.py:93
  114.3 1.3 fusion.46
  115.6 2.6 %fusion.7 = f32[128,2048]{1,0:T(8,128)} fusion(bf16[128,2048]{1,0:T(8,128)(2,1)S(1)} %copy-done.3, bf16[128,2048]{1,0:T(8,128)(2,1)S(1)} %all_gather.11, bf16[2048,128]{1,0:T(8,128)(2,1)} %param.34, f32[128,128]{1,0:T(8,128)S(1)} %fusion.46), kind=kOutput, calls=%fused_computation.15 | convolution fusion | flops 134316032 | bytes 2686976 | tf_op jit(solution)/shard_map/dot_general | solution.py:98
  118.3 2.6 %copy.32 = bf16[16,12,2048]{2,1,0:T(8,128)(2,1)} copy(bf16[16,12,2048]{2,0,1:T(8,128)(2,1)} %all-reduce.2.cloned.1.call-done) | data formatting | bytes 1572864 | tf_op jit(solution)/shard_map/psum | solution.py:127
  120.9 4.3 %all-to-all-start.1 = ((bf16[16,12,2048]{2,1,0:T(8,128)(2,1)}), bf16[16,12,2048]{2,1,0:T(8,128)(2,1)}, u32[]{:S(2)}, u32[]{:S(2)}) async-start(bf16[16,12,2048]{2,1,0:T(8,128)(2,1)} %copy.32), calls=%async_computation.1 | async-start | bytes 2097152 | tf_op jit(solution)/shard_map/all_to_all | solution.py:128
  125.3 0.1 reduce_sum.79
  125.5 0.1 fusion.12
  125.7 21.3 %all-to-all-done.1 = bf16[16,12,2048]{2,1,0:T(8,128)(2,1)} async-done(((bf16[16,12,2048]{2,1,0:T(8,128)(2,1)}), bf16[16,12,2048]{2,1,0:T(8,128)(2,1)}, u32[]{:S(2)}, u32[]{:S(2)}) %all-to-all-start.1) | async-done | bytes 786464 | tf_op jit(solution)/shard_map/all_to_all | solution.py:128
  147.0 1.7 copy.33
  148.6 2.5 %gather_fusion = bf16[96,2048]{1,0:T(8,128)(2,1)S(1)} fusion(bf16[16,12,2048]{2,0,1:T(8,128)(2,1)S(1)} %copy.33, s32[96]{0:T(128)S(1)} %bitcast.56), kind=kCustom, calls=%fused_computation | custom fusion | bytes 787200 | tf_op jit(solution)/shard_map/gather | solution.py:129
  151.2 0.1 reshape.182
  151.3 0.2 multiply_reduce_fusion
  151.6 42.5 %reduce-scatter.2.cloned.1.call-done = f32[8,2048]{1,0:T(8,128)} async-done(((f32[128,2048]{1,0:T(8,128)}), f32[8,2048]{1,0:T(8,128)}) %reduce-scatter.2.cloned.1.call-update) | async-done | bytes 65552 | tf_op jit(solution)/shard_map/reduce_scatter | solution.py:97
  194.0 1.0 fusion.41
  195.1 0.2 multiply_reduce_fusion.1
  195.3 0.7 multiply_convert_fusion
  (49 shorter events, 0.8 us)
Async XLA Ops:
  7.4 6.6 %copy-start = (bf16[8,256,512]{2,1,0:T(8,128)(2,1)S(1)}, bf16[8,256,512]{2,1,0:T(8,128)(2,1)}, u32[]{:S(2)}) copy-start(bf16[8,256,512]{2,1,0:T(8,128)(2,1)} %param.26) | copy-start | bytes 6291460
  7.4 8.1 %copy-start.8 = (bf16[8,512]{1,0:T(8,128)(2,1)S(1)}, bf16[8,512]{1,0:T(8,128)(2,1)}, u32[]{:S(2)}) copy-start(bf16[8,512]{1,0:T(8,128)(2,1)} %param.24) | copy-start | bytes 24580
  7.4 8.1 %copy-start.5 = (bf16[8,8,512]{2,1,0:T(8,128)(2,1)S(1)}, bf16[8,8,512]{2,1,0:T(8,128)(2,1)}, u32[]{:S(2)}) copy-start(bf16[8,8,512]{2,1,0:T(8,128)(2,1)} %param.22) | copy-start | bytes 196612
  7.4 8.7 %copy-start.4 = (bf16[8,256,32]{1,2,0:T(8,128)(2,1)S(1)}, bf16[8,256,32]{1,2,0:T(8,128)(2,1)}, u32[]{:S(2)}) copy-start(bf16[8,256,32]{1,2,0:T(8,128)(2,1)} %param.27) | copy-start | bytes 393220
  7.4 110.9 %all-reduce.2.cloned.1.call-start = ((), (), s32[]{:S(2)}) async-start(), calls=%async_computation.3 | async-start | bytes 1572864 | tf_op jit(solution)/shard_map/psum | solution.py:127
  13.9 3.1 %copy-start.2 = (bf16[512,8,64]{0,2,1:T(8,128)(2,1)S(1)}, bf16[512,8,64]{0,2,1:T(8,128)(2,1)}, u32[]{:S(2)}) copy-start(bf16[512,8,64]{0,2,1:T(8,128)(2,1)} %param.29) | copy-start | bytes 1572868
  15.5 1.9 copy-start.6
  16.6 3.1 %copy-start.9 = (bf16[2048]{0:T(1024)(128)(2,1)S(1)}, bf16[2048]{0:T(1024)(128)(2,1)}, u32[]{:S(2)}) copy-start(bf16[2048]{0:T(1024)(128)(2,1)} %param.31) | copy-start | bytes 12292
  67.6 3.8 %copy-start.1 = (bf16[1,256,2048]{2,1,0:T(8,128)(2,1)S(1)}, bf16[1,256,2048]{2,1,0:T(8,128)(2,1)}, u32[]{:S(2)}) copy-start(bf16[1,256,2048]{2,1,0:T(8,128)(2,1)} %param.40) | copy-start | bytes 3145732
  72.7 42.9 %copy-start.3 = (bf16[128,2048]{1,0:T(8,128)(2,1)S(1)}, bf16[128,2048]{1,0:T(8,128)(2,1)}, u32[]{:S(2)}) copy-start(bf16[128,2048]{1,0:T(8,128)(2,1)} %param.35) | copy-start | bytes 1572868
  72.7 121.3 %reduce-scatter.2.cloned.1.call-start = ((), (), s32[]{:S(2)}) async-start(), calls=%async_computation.4 | async-start | bytes 1114112 | tf_op jit(solution)/shard_map/reduce_scatter | solution.py:97
  118.2 7.0 %copy-start.10 = (bf16[2048]{0:T(1024)(128)(2,1)S(1)}, bf16[2048]{0:T(1024)(128)(2,1)}, u32[]{:S(2)}) copy-start(bf16[2048]{0:T(1024)(128)(2,1)} %param.32) | copy-start | bytes 12292
  118.3 7.1 %copy-start.11 = (bf16[2048]{0:T(1024)(128)(2,1)S(1)}, bf16[2048]{0:T(1024)(128)(2,1)}, u32[]{:S(2)}) copy-start(bf16[2048]{0:T(1024)(128)(2,1)} %param.41) | copy-start | bytes 12292
  118.3 7.1 %copy-start.7 = (f32[8,6]{1,0:T(8,128)S(1)}, f32[8,6]{1,0:T(8,128)}, u32[]{:S(2)}) copy-start(f32[8,6]{1,0:T(8,128)} %param.37) | copy-start | bytes 580
  120.9 26.0 %all-to-all-start.1 = ((bf16[16,12,2048]{2,1,0:T(8,128)(2,1)}), bf16[16,12,2048]{2,1,0:T(8,128)(2,1)}, u32[]{:S(2)}, u32[]{:S(2)}) async-start(bf16[16,12,2048]{2,1,0:T(8,128)(2,1)} %copy.32), calls=%async_computation.1 | async-start | bytes 2097152 | tf_op jit(solution)/shard_map/all_to_all | solution.py:128
Sparse Core Ops, SparseCore 0:
  72.8 17.2 all-reduce.1
Sparse Core Ops, SparseCore 1:
  118.3 75.6 reduce-scatter.1
where the time goes:
time: 204 us; the launch traced here: 203 us
  blocking collectives  80 us (39%)
  waiting for transfers between devices  63.8 us (31%)
  local copies, waits for them, and re-layouts  18.2 us (9%)
  between operations  15.1 us (7%)
  matrix products  14 us (7%)
  other arithmetic  7.9 us (4%)
  starting transfers between devices  4.41 us (2%)
    reduce_scatter x1, waiting for transfers between devices, on_device(): lax.psum_scatter(jnp.dot(hidden_all, dense_w_down, preferred_element_type...  42.5 us
    all_gather x1, blocking collectives, on_device(): piece = lax.all_gather(mixed, 'ep', axis=0, tiled=True)  41.5 us
    all_to_all x1, blocking collectives, on_device(): lax.all_to_all(outgoing, 'ep', split_axis=0, concat_axis=0, tiled=True)  34.6 us
    all_to_all x1, waiting for transfers between devices, on_device(): lax.all_to_all(summed, 'ep', split_axis=0, concat_axis=0, tiled=True)  21.3 us
    scatter x2, local copies, waits for them, and re-layouts, on_device(): outgoing.at[route_ids, slot_index]  9.47 us
    all_to_all x1, starting transfers between devices, on_device(): lax.all_to_all(summed, 'ep', split_axis=0, concat_axis=0, tiled=True)  4.34 us
  transfers between devices with their start and end apart: 3, of which 2 were waited for; matrix products, arithmetic and copies ran while one was open for 6% of the time, Pallas kernels for 0%

commit v1 on v0

v1 whole, which is shorter than its diff:
```python
import functools
import math

import jax
import jax.numpy as jnp
from jax import lax
from jax.experimental import pallas as pl
from jax.experimental.pallas import tpu as pltpu
from jax.sharding import PartitionSpec as P

NOPE = 64
ALPHA = 8.0**0.25
EPS = 1e-06
ROPE_BASE = 10000.0
F32 = jnp.float32
BF16 = jnp.bfloat16
MESH = pl.DeviceIdType.MESH
VMEM = pltpu.VMEM


def normalize(values, gain):
    center = jnp.mean(values, -1, keepdims=True)
    shifted = values - center
    spread = jnp.mean(jnp.square(shifted), -1, keepdims=True)
    return shifted * lax.rsqrt(spread + EPS) * gain


def silu(value):
    return value / (1.0 + jnp.exp(-value))


def dot(a, b):
    return jnp.dot(a, b, preferred_element_type=F32)


def dot_nt(a, b):
    return lax.dot_general(a, b, (((1,), (1,)), ((), ())), preferred_element_type=F32)


def kernel(
    n,
    lengths,
    residual,
    query_latent,
    query_rotary,
    latent_new,
    rotary_new,
    vecs,
    ids,
    route_scores,
    rotary_cache,
    cache_hbm,
    vu_hbm,
    op_hbm,
    eg_hbm,
    eu_hbm,
    dg_hbm,
    du_hbm,
    ed_hbm,
    dd_hbm,
    out,
    cache,
    vu,
    op,
    eg,
    eu,
    dg,
    du,
    ed,
    dd,
    lat,
    gath,
    pout,
    pin,
    sbuf,
    rbuf,
    cache_sem,
    w_sem,
    ag_send,
    ag_recv,
    fw_send,
    fw_recv,
    p_sem,
    rs_send,
    rs_recv,
):
    me = lax.axis_index("ep")
    core = lax.axis_index("tp")
    other = 1 - core
    seqs, width = residual.shape
    heads = query_latent.shape[1]
    rope = query_rotary.shape[-1]
    cache_len = cache.shape[1]
    extra = gath.shape[-1] - width
    experts = n

    cache_copies = [
        pltpu.make_async_copy(cache_hbm.at[s], cache.at[s], cache_sem.at[s]) for s in range(seqs)
    ]
    for c in cache_copies:
        c.start()
    pairs = [
        (vu_hbm, vu),
        (op_hbm, op),
        (eg_hbm.at[0], eg),
        (eu_hbm.at[0], eu),
        (dg_hbm, dg),
        (du_hbm, du),
        (ed_hbm.at[0], ed),
        (dd_hbm, dd),
    ]
    w_copies = [pltpu.make_async_copy(a, b, w_sem.at[k]) for k, (a, b) in enumerate(pairs)]
    for c in w_copies:
        c.start()

    barrier = pltpu.get_barrier_semaphore()

    def greet(d, carry):
        pl.semaphore_signal(
            barrier, inc=1, device_id={"ep": lax.rem(me + d, n)}, device_id_type=MESH
        )
        return carry

    lax.fori_loop(1, n, greet, 0)
    pl.semaphore_signal(barrier, inc=1, device_id={"tp": other}, device_id_type=MESH)

    half = rope // 2
    lane = lax.broadcasted_iota(jnp.int32, (seqs, rope), 1)
    row = lax.broadcasted_iota(jnp.int32, (seqs, rope), 0)
    pos = jnp.zeros((seqs, rope), F32)
    for s in range(seqs):
        pos = jnp.where(row == s, lengths[s].astype(F32), pos)
    inv_freq = jnp.exp(lax.rem(lane, half).astype(F32) * (-math.log(ROPE_BASE) / half))
    angles = pos * inv_freq
    cosine = jnp.cos(angles)
    sine = jnp.sin(angles)
    ra = lax.broadcasted_iota(jnp.int32, (rope, rope), 0)
    rb = lax.broadcasted_iota(jnp.int32, (rope, rope), 1)
    swap = jnp.where(ra + half == rb, 1.0, jnp.where(ra == rb + half, -1.0, 0.0)).astype(BF16)
    q_rot = query_rotary[...].astype(F32).reshape(seqs * heads, rope)
    q_swap = dot(q_rot.astype(BF16), swap).reshape(seqs, heads, rope)
    q_rot = q_rot.reshape(seqs, heads, rope)
    k_rot = rotary_new[...]
    k_turn = (k_rot.astype(F32) * cosine + dot(k_rot, swap) * sine).astype(BF16).astype(F32)
    ln_all = latent_new[...].astype(F32)
    score_scale = (NOPE + rope) ** (-0.5)
    t_idx = lax.broadcasted_iota(jnp.int32, (heads, cache_len), 1)

    for s in range(seqs):
        q_turn = (q_rot[s] * cosine[s : s + 1] + q_swap[s] * sine[s : s + 1]).astype(BF16)
        ql = query_latent[s]
        own = (
            jnp.sum(ql.astype(F32) * ln_all[s : s + 1], -1, keepdims=True)
            + jnp.sum(q_turn.astype(F32) * k_turn[s : s + 1], -1, keepdims=True)
        ) * score_scale
        rot_part = dot_nt(q_turn, rotary_cache[s])
        cache_copies[s].wait()
        block = cache[s]
        scores = (dot_nt(ql, block) + rot_part) * score_scale
        scores = jnp.where(t_idx < lengths[s], scores, -jnp.inf)
        top = jnp.maximum(jnp.max(scores, -1, keepdims=True), own)
        probs = jnp.exp(scores - top)
        own_p = jnp.exp(own - top)
        total = jnp.sum(probs, -1, keepdims=True) + own_p
        weights = (probs / total).astype(BF16)
        own_w = (own_p / total).astype(BF16).astype(F32)
        lat[s * heads : (s + 1) * heads, :] = dot(weights, block) + own_w * ln_all[s : s + 1]

    w_copies[0].wait()
    w_copies[1].wait()
    wide = dot(lat[...].astype(BF16), vu[...])
    vdim = wide.shape[1] // heads
    wide = wide.reshape(seqs, heads, wide.shape[1])
    h_row = lax.broadcasted_iota(jnp.int32, wide.shape, 1)
    h_lane = lax.broadcasted_iota(jnp.int32, wide.shape, 2)
    own_head = (h_lane >= h_row * vdim) & (h_lane < (h_row + 1) * vdim)
    heads_out = jnp.sum(jnp.where(own_head, wide, 0.0), 1).astype(BF16)
    attn = dot(heads_out, op[...]).astype(BF16).astype(F32)
    mixed = normalize(ALPHA * residual[...].astype(F32) + attn, vecs[0:1, :]).astype(BF16)
    mixed_f = mixed.astype(F32)
    mix = 1.0 / (1.0 + jnp.exp(-jnp.sum(mixed_f * vecs[1:2, :], -1, keepdims=True)))

    sc = route_scores[...]
    share = sc / jnp.sum(sc, -1, keepdims=True)
    e_lane = lax.broadcasted_iota(jnp.int32, (seqs, extra), 1)
    low = e_lane > experts
    e_idx = jnp.where(low, e_lane - (experts + 1), e_lane)
    coef = jnp.where(e_idx == experts, mix, 0.0)
    for k in range(ids.shape[1]):
        coef = coef + jnp.where(e_idx == ids[:, k : k + 1], share[:, k : k + 1], 0.0)
    high = coef.astype(BF16)
    coef = jnp.where(low, coef - high.astype(F32), high.astype(F32)).astype(BF16)
    mine = gath.at[core, me]
    mine[:, :width] = mixed
    mine[:, width:] = coef

    pl.semaphore_wait(barrier, n)

    def ag_copy(d, block, target):
        return pltpu.make_async_remote_copy(
            src_ref=gath.at[core, block],
            dst_ref=gath.at[core, block],
            send_sem=ag_send.at[d],
            recv_sem=ag_recv.at[d],
            device_id={"ep": target},
            device_id_type=MESH,
        )

    def fw_copy(d, half_idx, block):
        return pltpu.make_async_remote_copy(
            src_ref=gath.at[half_idx, block],
            dst_ref=gath.at[half_idx, block],
            send_sem=fw_send.at[d],
            recv_sem=fw_recv.at[d],
            device_id={"tp": other},
            device_id_type=MESH,
        )

    def ag_start(d, carry):
        ag_copy(d, me, lax.rem(me + d, n)).start()
        return carry

    lax.fori_loop(1, n, ag_start, 0)
    fw_copy(0, core, me).start()
    for c in w_copies[2:]:
        c.wait()

    def ag_forward(d, carry):
        src = lax.rem(me + n - d, n)
        ag_copy(d, src, me).wait_recv()
        fw_copy(d, core, src).start()
        return carry

    lax.fori_loop(1, n, ag_forward, 0)

    chunk = 16
    rows = chunk * seqs

    def load(half_idx, b):
        block = gath[half_idx, pl.ds(b * chunk, chunk)]
        flat = block.astype(F32).reshape(rows, width + extra)
        x = flat[:, :width].astype(BF16)
        tail = flat[:, width:]
        c_lane = lax.broadcasted_iota(jnp.int32, (rows, extra), 1)
        pick = (c_lane == me) | (c_lane == me + experts + 1)
        weight = jnp.sum(jnp.where(pick, tail, 0.0), -1, keepdims=True)
        pick = (c_lane == experts) | (c_lane == 2 * experts + 1)
        blend = jnp.sum(jnp.where(pick, tail, 0.0), -1, keepdims=True)
        return x, weight, blend

    def expert_hidden(x, weight):
        return (silu(dot(x, eg[...])) * dot(x, eu[...]) * weight).astype(BF16)

    tile = 512 if width % 512 == 0 else width

    def fw_wait(d, carry):
        fw_copy(d, other, lax.rem(me + n - d, n)).wait_recv()
        return carry

    def partner_rows(b, carry):
        x, weight, _ = load(other, b)
        hidden = expert_hidden(x, weight)
        for t in range(0, width, tile):
            part = dot(hidden, ed[:, t : t + tile])
            pout[pl.ds(b * chunk, chunk), :, t : t + tile] = part.reshape(
                chunk, seqs, tile
            ).astype(BF16)
        return carry

    lax.fori_loop(0, n, fw_wait, 0)
    lax.fori_loop(0, n // chunk, partner_rows, 0)
    p_copy = pltpu.make_async_remote_copy(
        src_ref=pout,
        dst_ref=pin,
        send_sem=p_sem.at[0],
        recv_sem=p_sem.at[1],
        device_id={"tp": other},
        device_id_type=MESH,
    )
    p_copy.start()

    def own_hidden(b):
        x, weight, blend = load(core, b)
        hidden = expert_hidden(x, weight)
        d_hidden = (silu(dot(x, dg[...])) * dot(x, du[...]) * blend).astype(BF16)
        return hidden, d_hidden

    def own_rows(b, carry):
        hidden, d_hidden = own_hidden(b)
        for t in range(0, width, tile):
            part = dot(hidden, ed[:, t : t + tile]) + dot(d_hidden, dd[:, t : t + tile])
            part = part.reshape(chunk, seqs, tile)
            part = part + pin[pl.ds(b * chunk, chunk), :, t : t + tile].astype(F32)
            sbuf[pl.ds(b * chunk, chunk), :, t : t + tile] = part.astype(BF16)
        return carry

    p_copy.wait_recv()
    lax.fori_loop(0, n // chunk, own_rows, 0)

    def rs_copy(d, block, slot, target):
        return pltpu.make_async_remote_copy(
            src_ref=sbuf.at[block],
            dst_ref=rbuf.at[slot],
            send_sem=rs_send.at[d],
            recv_sem=rs_recv.at[d],
            device_id={"ep": target},
            device_id_type=MESH,
        )

    def rs_start(d, carry):
        target = lax.rem(me + d, n)
        rs_copy(d, target, d, target).start()
        return carry

    lax.fori_loop(1, n, rs_start, 0)
    start = ALPHA * mixed_f + sbuf[me].astype(F32)

    def rs_add(d, total):
        rs_copy(d, me, d, me).wait_recv()
        return total + rbuf[d].astype(F32)

    total = lax.fori_loop(1, n, rs_add, start)
    out[...] = normalize(total, vecs[2:3, :]).astype(BF16)

    def drain(d, carry):
        ag_copy(d, me, me).wait_send()
        rs_copy(d, me, d, me).wait_send()
        return carry

    def drain_fw(d, carry):
        fw_copy(d, core, me).wait_send()
        return carry

    lax.fori_loop(1, n, drain, 0)
    lax.fori_loop(0, n, drain_fw, 0)
    p_copy.wait_send()


def on_device(
    n,
    residual,
    query_latent,
    query_rotary,
    latent_new,
    rotary_new,
    latent_cache,
    rotary_cache,
    lengths,
    value_up,
    out_proj,
    attn_gain,
    mix_gate,
    dense_w_gate,
    dense_w_up,
    dense_w_down,
    expert_ids,
    expert_scores,
    expert_gate,
    expert_up,
    expert_down,
    out_gain,
):
    seqs, width = residual.shape
    heads = query_latent.shape[1]
    vu = value_up.reshape(value_up.shape[0], -1)
    vecs = jnp.stack([attn_gain, mix_gate, out_gain]).astype(F32)
    extra = -(-2 * (n + 1) // 128) * 128
    vmem = pl.BlockSpec(memory_space=VMEM)
    hbm = pl.BlockSpec(memory_space=pl.ANY)
    smem = pl.BlockSpec(memory_space=pltpu.SMEM)
    dma = pltpu.SemaphoreType.DMA
    block = (n, seqs, width)
    return pl.pallas_call(
        functools.partial(kernel, n),
        out_shape=jax.ShapeDtypeStruct((seqs, width), BF16),
        in_specs=[smem] + [vmem] * 9 + [hbm] * 9,
        out_specs=vmem,
        scratch_shapes=[
            VMEM(latent_cache.shape, BF16),
            VMEM(vu.shape, BF16),
            VMEM(out_proj.shape, BF16),
            VMEM(expert_gate.shape[1:], BF16),
            VMEM(expert_up.shape[1:], BF16),
            VMEM(dense_w_gate.shape, BF16),
            VMEM(dense_w_up.shape, BF16),
            VMEM(expert_down.shape[1:], BF16),
            VMEM(dense_w_down.shape, BF16),
            VMEM((seqs * heads, latent_cache.shape[-1]), F32),
            VMEM((2, n, seqs, width + extra), BF16),
            VMEM(block, BF16),
            VMEM(block, BF16),
            VMEM(block, BF16),
            VMEM(block, BF16),
            dma((seqs,)),
            dma((8,)),
            dma((n,)),
            dma((n,)),
            dma((n,)),
            dma((n,)),
            dma((2,)),
            dma((n,)),
            dma((n,)),
        ],
        compiler_params=pltpu.CompilerParams(
            collective_id=0, has_side_effects=True, vmem_limit_bytes=60 * 1024 * 1024
        ),
    )(
        lengths,
        residual,
        query_latent,
        query_rotary,
        latent_new,
        rotary_new,
        vecs,
        expert_ids,
        expert_scores,
        rotary_cache,
        latent_cache,
        vu,
        out_proj,
        expert_gate,
        expert_up,
        dense_w_gate,
        dense_w_up,
        expert_down,
        dense_w_down,
    )


def solution(mesh):
    rows = P(("ep", "tp"), None)
    rows3 = P(("ep", "tp"), None, None)
    return jax.shard_map(
        functools.partial(on_device, mesh.shape["ep"]),
        mesh=mesh,
        in_specs=(
            rows,
            rows3,
            rows3,
            rows,
            rows,
            rows3,
            rows3,
            P(("ep", "tp")),
            P(),
            P(),
            P(),
            P(),
            P(None, "ep"),
            P(None, "ep"),
            P("ep", None),
            rows,
            rows,
            P("ep", None, "tp"),
            P("ep", None, "tp"),
            P("ep", "tp", None),
            P(),
        ),
        out_specs=rows,
        check_vma=False,
    )
```

time: 204 us -> 49.5 us (0.24)
  the two profiles are of different devices: /device:TPU:0 before, /device:TPU:28 now
where the time goes in v1:
time: 49.5 us; the launch traced here: 49.1 us
  Pallas kernels  41 us (83%)
  local copies, waits for them, and re-layouts  7.42 us (15%)
  other arithmetic  0.65 us (1%)
    pallas_call x1, Pallas kernels, on_device(): pl.pallas_call(functools.partial(kernel, n), out_shape=jax.ShapeDtypeStru...  41 us
    unnamed x2, local copies, waits for them, and re-layouts  3.28 us
    another operation x3, local copies, waits for them, and re-layouts, on_device(): vecs = jnp.stack([attn_gain, mix_gate, out_gain]).astype(F32)  2.08 us
    reshape x1, local copies, waits for them, and re-layouts, on_device(): vu = value_up.reshape(value_up.shape[0], -1)  2.06 us

profile of v1, /device:TPU:28, one launch (start us, length us, event | category | flops | bytes accessed | tf_op | source)
XLA Modules:
  0.0 49.1 jit_solution(18378629382469955915)
XLA Ops:
  0.0 0.7 %stack.12 = bf16[1,2048]{1,0:T(2,128)(2,1)S(1)} reshape(bf16[2048]{0:T(1024)(128)(2,1)} %param.31) | data formatting | bytes 8192 | tf_op jit(solution)/shard_map/stack | solution.py:366
  0.7 0.7 %stack.13 = bf16[1,2048]{1,0:T(2,128)(2,1)S(1)} reshape(bf16[2048]{0:T(1024)(128)(2,1)} %param.32) | data formatting | bytes 8192 | tf_op jit(solution)/shard_map/stack | solution.py:366
  1.4 0.7 %stack.14 = bf16[1,2048]{1,0:T(2,128)(2,1)S(1)} reshape(bf16[2048]{0:T(1024)(128)(2,1)} %param.41) | data formatting | bytes 8192 | tf_op jit(solution)/shard_map/stack | solution.py:366
  2.1 0.6 %maximum_convert_fusion.vecs = f32[3,2048]{1,0:T(4,128)} fusion(bf16[1,2048]{1,0:T(2,128)(2,1)S(1)} %stack.14, bf16[1,2048]{1,0:T(2,128)(2,1)S(1)} %stack.13, bf16[1,2048]{1,0:T(2,128)(2,1)S(1)} %stack.12), kind=kLoop, calls=%fused_computation | loop fusion | flops 36864 | bytes 36864 | tf_op jit(solution)/shard_map/convert_element_type | solution.py:366
  2.7 1.9 %copy.24.rotary_cache = bf16[8,256,32]{2,1,0:T(8,128)(2,1)} copy(bf16[8,256,32]{1,2,0:T(8,128)(2,1)} %param.27) | data formatting | bytes 262144 | tf_op args[6]
  4.6 2.1 %copy.25.vu_hbm = bf16[512,512]{1,0:T(8,128)(2,1)} copy(bf16[512,512]{0,1:T(8,128)(2,1)} %bitcast.1) | data formatting | bytes 1048576 | tf_op jit(solution)/shard_map/reshape | solution.py:365
  6.7 41.0 %shard_map.199 = bf16[8,2048]{1,0:T(8,128)(2,1)} custom-call(s32[8]{0:T(128)} %lengths.1, bf16[8,2048]{1,0:T(8,128)(2,1)} %residual.1, bf16[8,8,512]{2,1,0:T(8,128)(2,1)} %query_latent.1, bf16[8,8,32]{2,1,0:T(8,128)(2,1)} %query_rotary.1, bf16[8,512]{1,0:T(8,128)(2,1)} %latent_new.1, bf16[8,32]{1,0:T(8,128)(2,1)} %rotary_new.1, ...), custom_call_target="tpu_custom_call" | custom-call | tf_op jit(solution)/shard_map/pallas_call | solution.py:373
  47.7 1.4 %copy.27 = bf16[8,2048]{1,0:T(8,128)(2,1)} copy(bf16[8,2048]{1,0:T(8,128)(2,1)} %shard_map.199) | data formatting | bytes 65536

commit v2 on v1

--- a/solution.py
+++ b/solution.py
@@ -25,6 +25,17 @@
     return shifted * lax.rsqrt(spread + EPS) * gain
 
 
+def vector(ref):
+    return ref[...].astype(F32).reshape(1, ref.shape[0])
+
+
+def inner_size(n):
+    size = 1
+    while size * size < n:
+        size *= 2
+    return size if n % size == 0 else n
+
+
 def silu(value):
     return value / (1.0 + jnp.exp(-value))
 
@@ -45,7 +56,9 @@
     query_rotary,
     latent_new,
     rotary_new,
-    vecs,
+    attn_gain,
+    mix_gate,
+    out_gain,
     ids,
     route_scores,
     rotary_cache,
@@ -74,13 +87,18 @@
     pin,
     sbuf,
     rbuf,
+    zbuf,
+    hid_own,
+    hid_other,
+    hid_dense,
     cache_sem,
     w_sem,
     ag_send,
     ag_recv,
     fw_send,
     fw_recv,
-    p_sem,
+    p_send,
+    p_recv,
     rs_send,
     rs_recv,
 ):
@@ -115,13 +133,27 @@
 
     barrier = pltpu.get_barrier_semaphore()
 
-    def greet(d, carry):
-        pl.semaphore_signal(
-            barrier, inc=1, device_id={"ep": lax.rem(me + d, n)}, device_id_type=MESH
-        )
-        return carry
-
-    lax.fori_loop(1, n, greet, 0)
+    inner = inner_size(n)
+    outer = n // inner
+    zo = lax.div(me, inner)
+    xi = lax.rem(me, inner)
+
+    def ahead(dz, dx):
+        return lax.rem(zo + dz, outer) * inner + lax.rem(xi + dx, inner)
+
+    def behind(dz, dx):
+        return ahead(outer - dz, inner - dx)
+
+    def greet_outer(d, carry):
+        pl.semaphore_signal(barrier, inc=1, device_id={"ep": ahead(d, 0)}, device_id_type=MESH)
+        return carry
+
+    def greet_inner(d, carry):
+        pl.semaphore_signal(barrier, inc=1, device_id={"ep": ahead(0, d)}, device_id_type=MESH)
+        return carry
+
+    lax.fori_loop(1, outer, greet_outer, 0)
+    lax.fori_loop(1, inner, greet_inner, 0)
     pl.semaphore_signal(barrier, inc=1, device_id={"tp": other}, device_id_type=MESH)
 
     half = rope // 2
@@ -146,29 +178,33 @@
     score_scale = (NOPE + rope) ** (-0.5)
     t_idx = lax.broadcasted_iota(jnp.int32, (heads, cache_len), 1)
 
+    score_rows, own_rows_all = [], []
     for s in range(seqs):
         q_turn = (q_rot[s] * cosine[s : s + 1] + q_swap[s] * sine[s : s + 1]).astype(BF16)
         ql = query_latent[s]
-        own = (
+        own_rows_all.append(
             jnp.sum(ql.astype(F32) * ln_all[s : s + 1], -1, keepdims=True)
             + jnp.sum(q_turn.astype(F32) * k_turn[s : s + 1], -1, keepdims=True)
-        ) * score_scale
-        rot_part = dot_nt(q_turn, rotary_cache[s])
+        )
+        rot_part = dot(q_turn, rotary_cache[s])
         cache_copies[s].wait()
-        block = cache[s]
-        scores = (dot_nt(ql, block) + rot_part) * score_scale
-        scores = jnp.where(t_idx < lengths[s], scores, -jnp.inf)
-        top = jnp.maximum(jnp.max(scores, -1, keepdims=True), own)
-        probs = jnp.exp(scores - top)
-        own_p = jnp.exp(own - top)
-        total = jnp.sum(probs, -1, keepdims=True) + own_p
-        weights = (probs / total).astype(BF16)
-        own_w = (own_p / total).astype(BF16).astype(F32)
-        lat[s * heads : (s + 1) * heads, :] = dot(weights, block) + own_w * ln_all[s : s + 1]
+        part = dot_nt(ql, cache[s]) + rot_part
+        score_rows.append(jnp.where(t_idx < lengths[s], part, -jnp.inf))
+    own = jnp.concatenate(own_rows_all, 0) * score_scale
+    scores = jnp.concatenate(score_rows, 0) * score_scale
+    top = jnp.maximum(jnp.max(scores, -1, keepdims=True), own)
+    probs = jnp.exp(scores - top)
+    own_p = jnp.exp(own - top)
+    total = jnp.sum(probs, -1, keepdims=True) + own_p
+    weights = probs / total
+    own_w = (own_p / total).astype(BF16).astype(F32)
+    for s in range(seqs):
+        at = slice(s * heads, (s + 1) * heads)
+        lat[at, :] = dot(weights[at].astype(BF16), cache[s]) + own_w[at] * ln_all[s : s + 1]
 
     w_copies[0].wait()
     w_copies[1].wait()
-    wide = dot(lat[...].astype(BF16), vu[...])
+    wide = dot_nt(lat[...].astype(BF16), vu[...])
     vdim = wide.shape[1] // heads
     wide = wide.reshape(seqs, heads, wide.shape[1])
     h_row = lax.broadcasted_iota(jnp.int32, wide.shape, 1)
@@ -176,9 +212,9 @@
     own_head = (h_lane >= h_row * vdim) & (h_lane < (h_row + 1) * vdim)
     heads_out = jnp.sum(jnp.where(own_head, wide, 0.0), 1).astype(BF16)
     attn = dot(heads_out, op[...]).astype(BF16).astype(F32)
-    mixed = normalize(ALPHA * residual[...].astype(F32) + attn, vecs[0:1, :]).astype(BF16)
+    mixed = normalize(ALPHA * residual[...].astype(F32) + attn, vector(attn_gain)).astype(BF16)
     mixed_f = mixed.astype(F32)
-    mix = 1.0 / (1.0 + jnp.exp(-jnp.sum(mixed_f * vecs[1:2, :], -1, keepdims=True)))
+    mix = 1.0 / (1.0 + jnp.exp(-jnp.sum(mixed_f * vector(mix_gate), -1, keepdims=True)))
 
     sc = route_scores[...]
     share = sc / jnp.sum(sc, -1, keepdims=True)
@@ -194,14 +230,14 @@
     mine[:, :width] = mixed
     mine[:, width:] = coef
 
-    pl.semaphore_wait(barrier, n)
-
-    def ag_copy(d, block, target):
+    pl.semaphore_wait(barrier, outer + inner - 1)
+
+    def ag_copy(slot, block, target):
         return pltpu.make_async_remote_copy(
             src_ref=gath.at[core, block],
             dst_ref=gath.at[core, block],
-            send_sem=ag_send.at[d],
-            recv_sem=ag_recv.at[d],
+            send_sem=ag_send.at[slot],
+            recv_sem=ag_recv.at[slot],
             device_id={"ep": target},
             device_id_type=MESH,
         )
@@ -216,24 +252,44 @@
             device_id_type=MESH,
         )
 
-    def ag_start(d, carry):
-        ag_copy(d, me, lax.rem(me + d, n)).start()
-        return carry
-
-    lax.fori_loop(1, n, ag_start, 0)
+    def ag_outer(d, carry):
+        ag_copy(d * inner, me, ahead(d, 0)).start()
+        return carry
+
+    def ag_inner(dz, block):
+        def send(d, carry):
+            ag_copy(dz * inner + d, block, ahead(0, d)).start()
+            return carry
+
+        lax.fori_loop(1, inner, send, 0)
+
+    lax.fori_loop(1, outer, ag_outer, 0)
+    ag_inner(0, me)
     fw_copy(0, core, me).start()
-    for c in w_copies[2:]:
+
+    def ag_relay(dz, carry):
+        block = behind(dz, 0)
+        ag_copy(dz * inner, block, me).wait_recv()
+        ag_inner(dz, block)
+        fw_copy(dz * inner, core, block).start()
+        return carry
+
+    lax.fori_loop(1, outer, ag_relay, 0)
+
+    def ag_forward(dz, carry):
+        def one(dx, inside):
+            block = behind(dz, dx)
+            ag_copy(dz * inner + dx, block, me).wait_recv()
+            fw_copy(dz * inner + dx, core, block).start()
+            return inside
+
+        return lax.fori_loop(1, inner, one, carry)
+
+    lax.fori_loop(0, outer, ag_forward, 0)
+    for c in w_copies[2:6]:
         c.wait()
 
-    def ag_forward(d, carry):
-        src = lax.rem(me + n - d, n)
-        ag_copy(d, src, me).wait_recv()
-        fw_copy(d, core, src).start()
-        return carry
-
-    lax.fori_loop(1, n, ag_forward, 0)
-
-    chunk = 16
+    chunk = min(n, 16)
     rows = chunk * seqs
 
     def load(half_idx, b):
@@ -251,80 +307,133 @@
     def expert_hidden(x, weight):
         return (silu(dot(x, eg[...])) * dot(x, eu[...]) * weight).astype(BF16)
 
-    tile = 512 if width % 512 == 0 else width
+    def own_hidden(b, carry):
+        x, weight, blend = load(core, b)
+        at = pl.ds(b * rows, rows)
+        hid_own[at, :] = expert_hidden(x, weight)
+        hid_dense[at, :] = (silu(dot(x, dg[...])) * dot(x, du[...]) * blend).astype(BF16)
+        return carry
+
+    lax.fori_loop(0, n // chunk, own_hidden, 0)
 
     def fw_wait(d, carry):
-        fw_copy(d, other, lax.rem(me + n - d, n)).wait_recv()
-        return carry
-
-    def partner_rows(b, carry):
+        fw_copy(d, other, behind(lax.div(d, inner), lax.rem(d, inner))).wait_recv()
+        return carry
+
+    lax.fori_loop(0, n, fw_wait, 0)
+
+    def partner_hidden(b, carry):
         x, weight, _ = load(other, b)
-        hidden = expert_hidden(x, weight)
-        for t in range(0, width, tile):
-            part = dot(hidden, ed[:, t : t + tile])
-            pout[pl.ds(b * chunk, chunk), :, t : t + tile] = part.reshape(
-                chunk, seqs, tile
-            ).astype(BF16)
-        return carry
-
-    lax.fori_loop(0, n, fw_wait, 0)
-    lax.fori_loop(0, n // chunk, partner_rows, 0)
-    p_copy = pltpu.make_async_remote_copy(
-        src_ref=pout,
-        dst_ref=pin,
-        send_sem=p_sem.at[0],
-        recv_sem=p_sem.at[1],
-        device_id={"tp": other},
-        device_id_type=MESH,
-    )
-    p_copy.start()
-
-    def own_hidden(b):
-        x, weight, blend = load(core, b)
-        hidden = expert_hidden(x, weight)
-        d_hidden = (silu(dot(x, dg[...])) * dot(x, du[...]) * blend).astype(BF16)
-        return hidden, d_hidden
-
-    def own_rows(b, carry):
-        hidden, d_hidden = own_hidden(b)
-        for t in range(0, width, tile):
-            part = dot(hidden, ed[:, t : t + tile]) + dot(d_hidden, dd[:, t : t + tile])
-            part = part.reshape(chunk, seqs, tile)
-            part = part + pin[pl.ds(b * chunk, chunk), :, t : t + tile].astype(F32)
-            sbuf[pl.ds(b * chunk, chunk), :, t : t + tile] = part.astype(BF16)
-        return carry
-
-    p_copy.wait_recv()
-    lax.fori_loop(0, n // chunk, own_rows, 0)
-
-    def rs_copy(d, block, slot, target):
+        hid_other[pl.ds(b * rows, rows), :] = expert_hidden(x, weight)
+        return carry
+
+    lax.fori_loop(0, n // chunk, partner_hidden, 0)
+    for c in w_copies[6:]:
+        c.wait()
+    tiles, tile = sbuf.shape[0], sbuf.shape[-1]
+
+    def p_copy(t):
         return pltpu.make_async_remote_copy(
-            src_ref=sbuf.at[block],
-            dst_ref=rbuf.at[slot],
-            send_sem=rs_send.at[d],
-            recv_sem=rs_recv.at[d],
+            src_ref=pout.at[t],
+            dst_ref=pin.at[t],
+            send_sem=p_send.at[t],
+            recv_sem=p_recv.at[t],
+            device_id={"tp": other},
+            device_id_type=MESH,
+        )
+
+    def rs_inner(t, slot, block, target):
+        return pltpu.make_async_remote_copy(
+            src_ref=sbuf.at[t, block],
+            dst_ref=rbuf.at[t, slot],
+            send_sem=rs_send.at[t, slot],
+            recv_sem=rs_recv.at[t, slot],
             device_id={"ep": target},
             device_id_type=MESH,
         )
 
-    def rs_start(d, carry):
-        target = lax.rem(me + d, n)
-        rs_copy(d, target, d, target).start()
-        return carry
-
-    lax.fori_loop(1, n, rs_start, 0)
-    start = ALPHA * mixed_f + sbuf[me].astype(F32)
-
-    def rs_add(d, total):
-        rs_copy(d, me, d, me).wait_recv()
-        return total + rbuf[d].astype(F32)
-
-    total = lax.fori_loop(1, n, rs_add, start)
-    out[...] = normalize(total, vecs[2:3, :]).astype(BF16)
+    def rs_outer(t, d, target):
+        return pltpu.make_async_remote_copy(
+            src_ref=zbuf.at[t, d],
+            dst_ref=rbuf.at[t, d * inner],
+            send_sem=rs_send.at[t, d * inner],
+            recv_sem=rs_recv.at[t, d * inner],
+            device_id={"ep": target},
+            device_id_type=MESH,
+        )
+
+    for t in range(tiles):
+        cols = slice(t * tile, (t + 1) * tile)
+
+        def partner_rows(b, carry):
+            part = dot(hid_other[pl.ds(b * rows, rows), :], ed[:, cols])
+            pout[t, pl.ds(b * chunk, chunk)] = part.reshape(chunk, seqs, tile).astype(BF16)
+            return carry
+
+        lax.fori_loop(0, n // chunk, partner_rows, 0)
+        p_copy(t).start()
+
+    for t in range(tiles):
+        cols = slice(t * tile, (t + 1) * tile)
+        p_copy(t).wait_recv()
+
+        def own_rows(b, carry):
+            at = pl.ds(b * rows, rows)
+            part = dot(hid_own[at, :], ed[:, cols]) + dot(hid_dense[at, :], dd[:, cols])
+            part = part.reshape(chunk, seqs, tile)
+            part = part + pin[t, pl.ds(b * chunk, chunk)].astype(F32)
+            sbuf[t, pl.ds(b * chunk, chunk)] = part.astype(BF16)
+            return carry
+
+        lax.fori_loop(0, n // chunk, own_rows, 0)
+
+        def rs_start(k, carry):
+            dz = outer - 1 - k
+
+            def one(dx, inside):
+                rs_inner(t, dz * inner + dx, ahead(dz, dx), ahead(0, dx)).start()
+                return inside
+
+            return lax.fori_loop(1, inner, one, carry)
+
+        lax.fori_loop(0, outer, rs_start, 0)
+
+    def inner_sum(t, dz, start):
+        def one(dx, total):
+            rs_inner(t, dz * inner + dx, me, me).wait_recv()
+            return total + rbuf[t, dz * inner + dx].astype(F32)
+
+        return lax.fori_loop(1, inner, one, start)
+
+    for t in range(tiles):
+
+        def rs_relay(k, carry):
+            dz = outer - k
+            value = inner_sum(t, dz, sbuf[t, ahead(dz, 0)].astype(F32))
+            zbuf[t, dz] = value.astype(BF16)
+            rs_outer(t, dz, ahead(dz, 0)).start()
+            return carry
+
+        lax.fori_loop(1, outer, rs_relay, 0)
+
+    sums = []
+    for t in range(tiles):
+        cols = slice(t * tile, (t + 1) * tile)
+        start = ALPHA * mixed_f[:, cols] + sbuf[t, me].astype(F32)
+        value = inner_sum(t, 0, start)
+
+        def outer_add(d, total):
+            rs_outer(t, d, me).wait_recv()
+            return total + rbuf[t, d * inner].astype(F32)
+
+        sums.append(lax.fori_loop(1, outer, outer_add, value))
+    total = jnp.concatenate(sums, axis=-1)
+    out[...] = normalize(total, vector(out_gain)).astype(BF16)
 
     def drain(d, carry):
         ag_copy(d, me, me).wait_send()
-        rs_copy(d, me, d, me).wait_send()
+        for t in range(tiles):
+            rs_inner(t, d, me, me).wait_send()
         return carry
 
     def drain_fw(d, carry):
@@ -333,7 +442,8 @@
 
     lax.fori_loop(1, n, drain, 0)
     lax.fori_loop(0, n, drain_fw, 0)
-    p_copy.wait_send()
+    for t in range(tiles):
+        p_copy(t).wait_send()
 
 
 def on_device(
@@ -362,18 +472,20 @@
 ):
     seqs, width = residual.shape
     heads = query_latent.shape[1]
-    vu = value_up.reshape(value_up.shape[0], -1)
-    vecs = jnp.stack([attn_gain, mix_gate, out_gain]).astype(F32)
+    vu = value_up.transpose(1, 2, 0).reshape(-1, value_up.shape[0])
+    rotary_turned = rotary_cache.transpose(0, 2, 1)
     extra = -(-2 * (n + 1) // 128) * 128
     vmem = pl.BlockSpec(memory_space=VMEM)
     hbm = pl.BlockSpec(memory_space=pl.ANY)
     smem = pl.BlockSpec(memory_space=pltpu.SMEM)
     dma = pltpu.SemaphoreType.DMA
-    block = (n, seqs, width)
+    tile = 512 if width % 512 == 0 else width
+    tiles = width // tile
+    block = (tiles, n, seqs, tile)
     return pl.pallas_call(
         functools.partial(kernel, n),
         out_shape=jax.ShapeDtypeStruct((seqs, width), BF16),
-        in_specs=[smem] + [vmem] * 9 + [hbm] * 9,
+        in_specs=[smem] + [vmem] * 11 + [hbm] * 9,
         out_specs=vmem,
         scratch_shapes=[
             VMEM(latent_cache.shape, BF16),
@@ -391,15 +503,20 @@
             VMEM(block, BF16),
             VMEM(block, BF16),
             VMEM(block, BF16),
+            VMEM((tiles, n // inner_size(n), seqs, tile), BF16),
+            VMEM((n * seqs, expert_gate.shape[-1]), BF16),
+            VMEM((n * seqs, expert_gate.shape[-1]), BF16),
+            VMEM((n * seqs, dense_w_gate.shape[-1]), BF16),
             dma((seqs,)),
             dma((8,)),
             dma((n,)),
             dma((n,)),
             dma((n,)),
             dma((n,)),
-            dma((2,)),
-            dma((n,)),
-            dma((n,)),
+            dma((tiles,)),
+            dma((tiles,)),
+            dma((tiles, n)),
+            dma((tiles, n)),
         ],
         compiler_params=pltpu.CompilerParams(
             collective_id=0, has_side_effects=True, vmem_limit_bytes=60 * 1024 * 1024
@@ -411,10 +528,12 @@
         query_rotary,
         latent_new,
         rotary_new,
-        vecs,
+        attn_gain,
+        mix_gate,
+        out_gain,
         expert_ids,
         expert_scores,
-        rotary_cache,
+        rotary_turned,
         latent_cache,
         vu,
         out_proj,

time: 49.5 us -> 37.9 us (0.77)
  the two profiles are of different devices: /device:TPU:28 before, /device:TPU:0 now
where the time goes in v2:
time: 37.9 us; the launch traced here: 37.7 us
  Pallas kernels  36.3 us (96%)
  local copies, waits for them, and re-layouts  1.38 us (4%)
    pallas_call x1, Pallas kernels, on_device(): pl.pallas_call(functools.partial(kernel, n), out_shape=jax.ShapeDtypeStru...  36.3 us
    unnamed x1, local copies, waits for them, and re-layouts  1.38 us

profile of v2, /device:TPU:0, one launch (start us, length us, event | category | flops | bytes accessed | tf_op | source)
XLA Modules:
  0.0 37.7 jit_solution(3475972657205895654)
XLA Ops:
  0.0 36.3 %shard_map.199 = bf16[8,2048]{1,0:T(8,128)(2,1)} custom-call(s32[8]{0:T(128)} %lengths.1, bf16[8,2048]{1,0:T(8,128)(2,1)} %residual.1, bf16[8,8,512]{2,1,0:T(8,128)(2,1)} %query_latent.1, bf16[8,8,32]{2,1,0:T(8,128)(2,1)} %query_rotary.1, bf16[8,512]{1,0:T(8,128)(2,1)} %latent_new.1, bf16[8,32]{1,0:T(8,128)(2,1)} %rotary_new.1, bf16[2048]{0:T(1024)(128)(2,1)} %attn_gain.1, ...), custom_call_target="tpu_custom_call" | custom-call | tf_op jit(solution)/shard_map/pallas_call | solution.py:485
  36.3 1.4 %copy.23 = bf16[8,2048]{1,0:T(8,128)(2,1)} copy(bf16[8,2048]{1,0:T(8,128)(2,1)} %shard_map.199) | data formatting | bytes 65536
